TPU v7x, 32 devices: a whole 2x2x4 slice. The times are simulated.
32 devices in a mesh: grp: 2 (over y), fs: 4 (over z), tp: 4 (over x, core).
Axes of the slice: x: 2, y: 2, z: 4, core: 2. Of those that a mesh axis runs over, the one named last changes fastest.
Arguments:
- tokens: bfloat16 [8, 384, 2048], P(('grp', 'fs'), None, 'tp'), parts along dimension 0, may hold values from -24 to 24
- input_gain: float32 [2048], replicated, may hold values from 0.1 to 1.9
- query_weight: bfloat16 [2048, 1024], P('fs', 'tp'), may hold values from -0.125 to 0.125
- key_weight: bfloat16 [2048, 1024], P('fs', 'tp'), may hold values from -0.125 to 0.125
- value_weight: bfloat16 [2048, 1024], P('fs', 'tp'), may hold values from -0.125 to 0.125
- output_gate_matrix: bfloat16 [2048, 1024], P('fs', 'tp'), may hold values from -0.125 to 0.125
- forward_decay: float32 [16], P('tp'), may hold values from -1 to 9
- backward_decay: float32 [16], P('tp'), may hold values from -1 to 9
- merge_weight: bfloat16 [1024, 2048], P('tp', 'fs'), may hold values from -0.375 to 0.375
- middle_gain: float32 [2048], replicated, may hold values from 0.1 to 1.9
- gate_weight: bfloat16 [2048, 5120], P('fs', 'tp'), may hold values from -0.125 to 0.125
- up_weight: bfloat16 [2048, 5120], P('fs', 'tp'), may hold values from -0.125 to 0.125
- down_weight: bfloat16 [5120, 2048], P('tp', 'fs'), may hold values from -0.15625 to 0.15625
Outputs:
- layer_out: bfloat16 [8, 384, 2048], P(('grp', 'fs'), None, 'tp'), parts along dimension 0
There are 2 independent parts, one for each index of `grp`. A program takes and returns all parts, laid end to end along the dimension named above; an argument that names none is the same for every part. Nothing has to cross between parts.
All inputs are finite; a program needn't handle non-finite values.
Results may differ from a plain program's by a relative error of at most 0.019.
Values may be sent and summed in bfloat16 or wider, within the bound.
A program may use at most 64 MiB of HBM per device.

v0:
```python
import jax
import jax.numpy as jnp
from jax import lax
from jax.sharding import PartitionSpec as P

BLOCK = 128
norm_eps = 1e-06
group_eps = 1e-05
rope_base = 10000.0
highest_precision = lax.Precision.HIGHEST


def rms_scale(values, gain_vector):
    widened = values.astype(jnp.float32)
    scaled = widened * lax.rsqrt(jnp.mean(widened * widened, axis=-1, keepdims=True) + norm_eps)
    return (scaled * gain_vector).astype(jnp.bfloat16)


def apply_rotary_heads(values, length):
    half_dim = values.shape[-1] // 2
    inverse = rope_base ** (-jnp.arange(half_dim, dtype=jnp.float32) / half_dim)
    angles = jnp.arange(length, dtype=jnp.float32)[:, None] * inverse[None, :]
    cosine = jnp.cos(angles)[:, None, :]
    sine_part = jnp.sin(angles)[:, None, :]
    lower_half = values[..., :half_dim]
    upper_half = values[..., half_dim:]
    return jnp.concatenate(
        [
            lower_half * cosine - upper_half * sine_part,
            upper_half * cosine + lower_half * sine_part,
        ],
        axis=-1,
    )


def carry_states(key_blocks, value_blocks, weighting, log_rates, block_size, backward):
    block_terms = jnp.einsum(
        "sbmhd,sbmhe->bshde",
        key_blocks * weighting[None, None, :, :, None],
        value_blocks,
        precision=highest_precision,
    )
    factor = jnp.exp(log_rates * block_size)[None, :, None, None]

    def advance(running, addend):
        return (running * factor + addend, running)

    initial = jnp.zeros(block_terms.shape[1:], jnp.float32)
    return lax.scan(advance, initial, block_terms, reverse=backward)[1]


def retain_blocks(
    query_rows, key_rows, value_rows, gate_rows, forward_decay, backward_decay, seq_count, length
):
    head_count = forward_decay.shape[0]
    head_dim = query_rows.shape[1] // head_count
    block_size = BLOCK
    block_count = length // block_size

    def split_heads(rows_in):
        return rows_in.astype(jnp.float32).reshape(seq_count, length, head_count, head_dim)

    def blocked(tensor):
        return tensor.reshape(seq_count, block_count, block_size, head_count, head_dim)

    queries = blocked(apply_rotary_heads(split_heads(query_rows), length))
    key_heads = blocked(apply_rotary_heads(split_heads(key_rows), length) * head_dim ** (-0.5))
    valued = blocked(split_heads(value_rows))
    rate_ahead = jax.nn.log_sigmoid(forward_decay)
    rate_behind = jax.nn.log_sigmoid(backward_decay)
    position = jnp.arange(block_size, dtype=jnp.float32)
    offset = position[:, None] - position[None, :]
    inside = jnp.where(
        offset[None] >= 0,
        jnp.exp(rate_ahead[:, None, None] * jnp.maximum(offset, 0.0)[None]),
        jnp.exp(rate_behind[:, None, None] * jnp.maximum(-offset, 0.0)[None]),
    )
    attention_scores = (
        jnp.einsum("sbchd,sbmhd->sbhcm", queries, key_heads, precision=highest_precision)
        * inside[None, None]
    )
    result = jnp.einsum("sbhcm,sbmhd->sbchd", attention_scores, valued, precision=highest_precision)
    column = position[:, None]
    key_ahead = jnp.exp(rate_ahead[None, :] * (block_size - 1 - column))
    query_ahead = jnp.exp(rate_ahead[None, :] * (column + 1))
    key_behind = jnp.exp(rate_behind[None, :] * column)
    query_behind = jnp.exp(rate_behind[None, :] * (block_size - column))
    from_before = carry_states(key_heads, valued, key_ahead, rate_ahead, block_size, False)
    from_after = carry_states(key_heads, valued, key_behind, rate_behind, block_size, True)
    result = (
        result
        + jnp.einsum("sbchd,bshde->sbche", queries, from_before, precision=highest_precision)
        * query_ahead[None, None, :, :, None]
    )
    result = (
        result
        + jnp.einsum("sbchd,bshde->sbche", queries, from_after, precision=highest_precision)
        * query_behind[None, None, :, :, None]
    )
    result = result.reshape(seq_count, length, head_count, head_dim)
    center = jnp.mean(result, axis=-1, keepdims=True)
    spread = jnp.mean(jnp.square(result - center), axis=-1, keepdims=True)
    normalized = (result - center) * lax.rsqrt(spread + group_eps)
    gated = jax.nn.silu(split_heads(gate_rows)) * normalized
    return gated.reshape(seq_count * length, head_count * head_dim).astype(jnp.bfloat16)


def accumulate(pieces, source):
    return tuple(
        (
            jnp.dot(source, weight_piece, preferred_element_type=jnp.float32)
            for weight_piece in pieces
        )
    )


def on_device(
    tokens,
    input_gain,
    query_weight,
    key_weight,
    value_weight,
    output_gate_matrix,
    forward_decay,
    backward_decay,
    merge_weight,
    middle_gain,
    gate_weight,
    up_weight,
    down_weight,
):
    seq_count, length, part_width = tokens.shape
    row_count = seq_count * length
    gathered = lax.all_gather(tokens, "tp", axis=2, tiled=True)
    normed = rms_scale(gathered.reshape(row_count, gathered.shape[2]), input_gain)
    query_sum, key_sum, value_sum, gating_sum = accumulate(
        (
            lax.all_gather(query_weight, "fs", axis=0, tiled=True),
            lax.all_gather(key_weight, "fs", axis=0, tiled=True),
            lax.all_gather(value_weight, "fs", axis=0, tiled=True),
            lax.all_gather(output_gate_matrix, "fs", axis=0, tiled=True),
        ),
        normed,
    )
    mixed = retain_blocks(
        query_sum.astype(jnp.bfloat16),
        key_sum.astype(jnp.bfloat16),
        value_sum.astype(jnp.bfloat16),
        gating_sum.astype(jnp.bfloat16),
        forward_decay,
        backward_decay,
        seq_count,
        length,
    )
    merge_term = jnp.dot(
        mixed,
        lax.all_gather(merge_weight, "fs", axis=1, tiled=True),
        preferred_element_type=jnp.float32,
    )
    merged = lax.psum_scatter(
        merge_term.astype(jnp.bfloat16), "tp", scatter_dimension=1, tiled=True
    ).astype(jnp.float32)
    middle = (tokens.reshape(row_count, part_width).astype(jnp.float32) + merged).astype(
        jnp.bfloat16
    )
    gathered_mid = lax.all_gather(middle, "tp", axis=1, tiled=True)
    normed_mid = rms_scale(gathered_mid, middle_gain)
    gate_full, up_full = (
        lax.all_gather(gate_weight, "fs", axis=0, tiled=True),
        lax.all_gather(up_weight, "fs", axis=0, tiled=True),
    )
    gate_act = jnp.dot(normed_mid, gate_full, preferred_element_type=jnp.float32)
    up_act = jnp.dot(normed_mid, up_full, preferred_element_type=jnp.float32)
    hidden = (jax.nn.silu(gate_act) * up_act).astype(jnp.bfloat16)
    down_term = jnp.dot(
        hidden,
        lax.all_gather(down_weight, "fs", axis=1, tiled=True),
        preferred_element_type=jnp.float32,
    )
    summed = lax.psum_scatter(
        down_term.astype(jnp.bfloat16), "tp", scatter_dimension=1, tiled=True
    ).astype(jnp.float32)
    layer_out = (middle.astype(jnp.float32) + summed).astype(jnp.bfloat16)
    return layer_out.reshape(seq_count, length, part_width)


def solution(mesh):
    placed = (
        P(("grp", "fs"), None, "tp"),
        P(),
        P("fs", "tp"),
        P("fs", "tp"),
        P("fs", "tp"),
        P("fs", "tp"),
        P("tp"),
        P("tp"),
        P("tp", "fs"),
        P(),
        P("fs", "tp"),
        P("fs", "tp"),
        P("tp", "fs"),
    )
    return jax.shard_map(
        on_device,
        mesh=mesh,
        in_specs=placed,
        out_specs=P(("grp", "fs"), None, "tp"),
        check_vma=False,
    )
```

profile of v0, /device:TPU:0, one launch (start us, length us, event | category | flops | bytes accessed | tf_op | source)
XLA Modules:
  0.0 571.5 jit_solution(758774433648440747)
XLA Ops:
  13.1 18.2 %all-gather.11.cloned.1.call-done = bf16[1,384,2048]{2,1,0:T(8,128)(2,1)} async-done(((bf16[1,384,512]{2,1,0:T(8,128)(2,1)}), bf16[1,384,2048]{2,1,0:T(8,128)(2,1)}) %all-gather.11.cloned.1.call-update) | async-done | bytes 1572880 | tf_op jit(solution)/shard_map/all_gather | solution.py:134
  31.3 1.9 fusion.3
  33.2 27.7 %all-gather.17.cloned.1.call-done = bf16[2048,256]{1,0:T(8,128)(2,1)} async-done(((bf16[512,256]{1,0:T(8,128)(2,1)}), bf16[2048,256]{1,0:T(8,128)(2,1)}) %all-gather.17.cloned.1.call-update) | async-done | bytes 1048592 | tf_op jit(solution)/shard_map/all_gather | solution.py:138
  60.9 2.6 convolution_convert_fusion.3
  63.5 26.4 %all-gather.19.cloned.1.call-done = bf16[2048,256]{1,0:T(8,128)(2,1)} async-done(((bf16[512,256]{1,0:T(8,128)(2,1)}), bf16[2048,256]{1,0:T(8,128)(2,1)}) %all-gather.19.cloned.1.call-update) | async-done | bytes 1048592 | tf_op jit(solution)/shard_map/all_gather | solution.py:139
  89.8 2.1 convolution_convert_fusion.2
  93.0 1.7 concatenate.22
  96.0 22.7 %all-gather.15.cloned.1.call-done = bf16[2048,256]{1,0:T(8,128)(2,1)} async-done(((bf16[512,256]{1,0:T(8,128)(2,1)}), bf16[2048,256]{1,0:T(8,128)(2,1)}) %all-gather.15.cloned.1.call-update) | async-done | bytes 1048592 | tf_op jit(solution)/shard_map/all_gather | solution.py:140
  118.6 2.6 convolution_convert_fusion.4
  126.3 1.4 convolution_multiply_fusion.1
  130.8 16.7 %all-gather.13.cloned.1.call-done = bf16[2048,256]{1,0:T(8,128)(2,1)} async-done(((bf16[512,256]{1,0:T(8,128)(2,1)}), bf16[2048,256]{1,0:T(8,128)(2,1)}) %all-gather.13.cloned.1.call-update) | async-done | bytes 1048592 | tf_op jit(solution)/shard_map/all_gather | solution.py:141
  147.4 28.8 %all-gather.21.cloned.1.call-done = bf16[256,2048]{1,0:T(8,128)(2,1)} async-done(((bf16[256,512]{1,0:T(8,128)(2,1)}), bf16[256,2048]{1,0:T(8,128)(2,1)}) %all-gather.21.cloned.1.call-update) | async-done | bytes 1048592 | tf_op jit(solution)/shard_map/all_gather | solution.py:157
  176.3 4.7 convolution_convert_fusion.1
  181.1 27.5 %reduce-scatter.3.cloned.1.call-done = bf16[384,512]{1,0:T(8,128)(2,1)} async-done(((bf16[384,2048]{1,0:T(8,128)(2,1)}), bf16[384,512]{1,0:T(8,128)(2,1)}) %reduce-scatter.3.cloned.1.call-update) | async-done | bytes 393232 | tf_op jit(solution)/shard_map/reduce_scatter | solution.py:160
  208.5 1.8 fusion.12
  212.7 17.5 %all-gather.23.cloned.1.call-done = bf16[384,2048]{1,0:T(8,128)(2,1)} async-done(((bf16[384,512]{1,0:T(8,128)(2,1)}), bf16[384,2048]{1,0:T(8,128)(2,1)}) %all-gather.23.cloned.1.call-update) | async-done | bytes 1572880 | tf_op jit(solution)/shard_map/all_gather | solution.py:166
  230.2 1.8 fusion
  232.0 97.8 %all-gather.25.cloned.1.call-done = bf16[2048,1280]{1,0:T(8,128)(2,1)} async-done(((bf16[512,1280]{1,0:T(8,128)(2,1)}), bf16[2048,1280]{1,0:T(8,128)(2,1)}) %all-gather.25.cloned.1.call-update) | async-done | bytes 5242896 | tf_op jit(solution)/shard_map/all_gather | solution.py:169
  329.8 6.5 %fusion.15 = f32[384,1280]{1,0:T(8,128)} fusion(bf16[2048,1280]{1,0:T(8,128)(2,1)} %all-gather.25.cloned.1.call-done, bf16[384,2048]{1,0:T(8,128)(2,1)} %all-gather.23.cloned.1.call-done, f32[2048]{0:T(1024)S(1)} %copy-done.12, f32[384]{0:T(512)S(1)} %add_rsqrt_fusion), kind=kOutput, calls=%fused_computation.36 | convolution fusion | flops 2016411648 | bytes 8791552 | tf_op jit(solution)/shard_map/dot_general | solution.py:172
  336.4 91.3 %all-gather.27.cloned.1.call-done = bf16[2048,1280]{1,0:T(8,128)(2,1)} async-done(((bf16[512,1280]{1,0:T(8,128)(2,1)}), bf16[2048,1280]{1,0:T(8,128)(2,1)}) %all-gather.27.cloned.1.call-update) | async-done | bytes 5242896 | tf_op jit(solution)/shard_map/all_gather | solution.py:170
  427.7 98.0 %all-gather.29.cloned.1.call-done = bf16[1280,2048]{1,0:T(8,128)(2,1)} async-done(((bf16[1280,512]{1,0:T(8,128)(2,1)}), bf16[1280,2048]{1,0:T(8,128)(2,1)}) %all-gather.29.cloned.1.call-update) | async-done | bytes 5242896 | tf_op jit(solution)/shard_map/all_gather | solution.py:177
  525.6 10.7 %convolution_convert_fusion = bf16[384,2048]{1,0:T(8,128)(2,1)} fusion(bf16[1280,2048]{1,0:T(8,128)(2,1)} %all-gather.29.cloned.1.call-done, bf16[2048,1280]{1,0:T(8,128)(2,1)} %all-gather.27.cloned.1.call-done, f32[384,1280]{1,0:T(8,128)} %fusion.15, bf16[384,2048]{1,0:T(8,128)(2,1)S(1)} %copy-done.3, f32[2048]{0:T(1024)S(1)} %copy-done.12, ...), kind=kOutput, calls=%fused_computation.15 | convolution fusion | flops 4033413120 | bytes 15607296 | tf_op jit(solution)/shard_map/dot_general | solution.py:175
  536.3 26.5 %reduce-scatter.5.cloned.1.call-done = bf16[384,512]{1,0:T(8,128)(2,1)} async-done(((bf16[384,2048]{1,0:T(8,128)(2,1)}), bf16[384,512]{1,0:T(8,128)(2,1)}) %reduce-scatter.5.cloned.1.call-update) | async-done | bytes 393232 | tf_op jit(solution)/shard_map/reduce_scatter | solution.py:180
  562.8 1.8 fusion.17
  (105 shorter events, 19.6 us)
Async XLA Ops:
  6.5 54.3 %copy-start.10 = (f32[2048]{0:T(1024)S(1)}, f32[2048]{0:T(1024)}, u32[]{:S(2)}) copy-start(f32[2048]{0:T(1024)} %param.18) | copy-start | bytes 24580
  6.5 24.7 %all-gather.11.cloned.1.call-start = ((), (), s32[]{:S(2)}) async-start(), calls=%async_computation.2 | async-start | bytes 1966080 | tf_op jit(solution)/shard_map/all_gather | solution.py:134
  7.3 53.6 %all-gather.17.cloned.1.call-start = ((), (), s32[]{:S(2)}) async-start(), calls=%async_computation.5 | async-start | bytes 1310720 | tf_op jit(solution)/shard_map/all_gather | solution.py:138
  8.0 81.8 %all-gather.19.cloned.1.call-start = ((), (), s32[]{:S(2)}) async-start(), calls=%async_computation.6 | async-start | bytes 1310720 | tf_op jit(solution)/shard_map/all_gather | solution.py:139
  8.7 109.9 %all-gather.15.cloned.1.call-start = ((), (), s32[]{:S(2)}) async-start(), calls=%async_computation.4 | async-start | bytes 1310720 | tf_op jit(solution)/shard_map/all_gather | solution.py:140
  9.3 138.1 %all-gather.13.cloned.1.call-start = ((), (), s32[]{:S(2)}) async-start(), calls=%async_computation.3 | async-start | bytes 1310720 | tf_op jit(solution)/shard_map/all_gather | solution.py:141
  9.9 166.4 %all-gather.21.cloned.1.call-start = ((), (), s32[]{:S(2)}) async-start(), calls=%async_computation.7 | async-start | bytes 1310720 | tf_op jit(solution)/shard_map/all_gather | solution.py:157
  10.5 198.1 %reduce-scatter.3.cloned.1.call-start = ((), (), s32[]{:S(2)}) async-start(), calls=%async_computation.8 | async-start | bytes 1966080 | tf_op jit(solution)/shard_map/reduce_scatter | solution.py:160
  31.3 58.6 %copy-start.1 = (bf16[1,384,2048]{2,1,0:T(8,128)(2,1)S(1)}, bf16[1,384,2048]{2,1,0:T(8,128)(2,1)}, u32[]{:S(2)}) copy-start(bf16[1,384,2048]{2,1,0:T(8,128)(2,1)} %all-gather.11.cloned.1.call-done) | copy-start | bytes 4718596
  33.2 58.7 %copy-start.8 = (f32[384]{0:T(512)}, f32[384]{0:T(512)S(1)}, u32[]{:S(2)}) copy-start(f32[384]{0:T(512)S(1)} %add_rsqrt_fusion.1) | copy-start | bytes 4612
  95.9 26.7 %copy-start.6 = (f32[128,4]{0,1:T(4,128)S(1)}, f32[128,4]{0,1:T(4,128)}, u32[]{:S(2)}) copy-start(f32[128,4]{0,1:T(4,128)} %get-tuple-element.231) | copy-start | bytes 6148
  95.9 26.7 %copy-start.7 = (f32[128,4]{0,1:T(4,128)S(1)}, f32[128,4]{0,1:T(4,128)}, u32[]{:S(2)}) copy-start(f32[128,4]{0,1:T(4,128)} %get-tuple-element.229) | copy-start | bytes 6148
  127.8 48.5 %copy-start.2 = (bf16[1,384,2048]{2,1,0:T(8,128)(2,1)S(1)}, bf16[1,384,2048]{2,1,0:T(8,128)(2,1)}, u32[]{:S(2)}) copy-start(bf16[1,384,2048]{2,1,0:T(8,128)(2,1)} %all-gather.11.cloned.1.call-done) | copy-start | bytes 4718596
  127.8 48.5 %copy-start.9 = (f32[384]{0:T(512)S(1)}, f32[384]{0:T(512)}, u32[]{:S(2)}) copy-start(f32[384]{0:T(512)} %copy-done.8) | copy-start | bytes 4612
  127.8 48.5 %copy-start.11 = (f32[2048]{0:T(1024)S(1)}, f32[2048]{0:T(1024)}, u32[]{:S(2)}) copy-start(f32[2048]{0:T(1024)} %param.18) | copy-start | bytes 24580
  130.7 77.8 %copy-start.4 = (bf16[1,384,512]{2,1,0:T(8,128)(2,1)S(1)}, bf16[1,384,512]{2,1,0:T(8,128)(2,1)}, u32[]{:S(2)}) copy-start(bf16[1,384,512]{2,1,0:T(8,128)(2,1)} %param.17) | copy-start | bytes 1179652
  181.0 49.2 %all-gather.23.cloned.1.call-start = ((), (), s32[]{:S(2)}) async-start(), calls=%async_computation.9 | async-start | bytes 1966080 | tf_op jit(solution)/shard_map/all_gather | solution.py:166
  210.4 119.5 %copy-start.12 = (f32[2048]{0:T(1024)S(1)}, f32[2048]{0:T(1024)}, u32[]{:S(2)}) copy-start(f32[2048]{0:T(1024)} %param.26) | copy-start | bytes 24580
  210.4 119.4 %all-gather.25.cloned.1.call-start = ((), (), s32[]{:S(2)}) async-start(), calls=%async_computation.10 | async-start | bytes 6553600 | tf_op jit(solution)/shard_map/all_gather | solution.py:169
  211.1 216.5 %all-gather.27.cloned.1.call-start = ((), (), s32[]{:S(2)}) async-start(), calls=%async_computation.11 | async-start | bytes 6553600 | tf_op jit(solution)/shard_map/all_gather | solution.py:170
  211.7 313.9 %all-gather.29.cloned.1.call-start = ((), (), s32[]{:S(2)}) async-start(), calls=%async_computation.12 | async-start | bytes 6553600 | tf_op jit(solution)/shard_map/all_gather | solution.py:177
  212.5 350.4 %reduce-scatter.5.cloned.1.call-start = ((), (), s32[]{:S(2)}) async-start(), calls=%async_computation.13 | async-start | bytes 1966080 | tf_op jit(solution)/shard_map/reduce_scatter | solution.py:180
  232.0 293.6 %copy-start.3 = (bf16[384,2048]{1,0:T(8,128)(2,1)S(1)}, bf16[384,2048]{1,0:T(8,128)(2,1)}, u32[]{:S(2)}) copy-start(bf16[384,2048]{1,0:T(8,128)(2,1)} %all-gather.23.cloned.1.call-done) | copy-start | bytes 4718596
  336.4 226.4 %copy-start = (bf16[384,512]{1,0:T(8,128)(2,1)S(1)}, bf16[384,512]{1,0:T(8,128)(2,1)}, u32[]{:S(2)}) copy-start(bf16[384,512]{1,0:T(8,128)(2,1)} %fusion.12) | copy-start | bytes 1179652
  (1 other events, 26.7 us)
Sparse Core Ops, SparseCore 0:
  8.9 22.3 all-gather.10
  32.8 27.9 all-gather.16
  62.4 27.3 all-gather.18
  91.3 27.3 all-gather.14
  120.1 27.3 all-gather.12
  148.9 27.3 all-gather.20
  181.1 27.3 reduce-scatter.2
  210.5 19.6 all-gather.22
  231.8 98.0 all-gather.24
  331.3 96.3 all-gather.26
  429.2 96.3 all-gather.28
  536.5 26.3 reduce-scatter.4
where the time goes:
time: 572 us; the launch traced here: 571 us
  waiting for transfers between devices  505 us (88%)
  matrix products  33.9 us (6%)
  between operations  13.9 us (2%)
  other arithmetic  12.9 us (2%)
    all_gather x1, waiting for transfers between devices, on_device(): lax.all_gather(down_weight, 'fs', axis=1, tiled=True)  98 us
    all_gather x1, waiting for transfers between devices, on_device(): lax.all_gather(gate_weight, 'fs', axis=0, tiled=True)  97.8 us
    all_gather x1, waiting for transfers between devices, on_device(): lax.all_gather(up_weight, 'fs', axis=0, tiled=True)  91.3 us
    all_gather x1, waiting for transfers between devices, on_device(): lax.all_gather(merge_weight, 'fs', axis=1, tiled=True)  28.8 us
    all_gather x1, waiting for transfers between devices, on_device(): lax.all_gather(query_weight, 'fs', axis=0, tiled=True)  27.7 us
    reduce_scatter x1, waiting for transfers between devices, on_device(): lax.psum_scatter(merge_term.astype(jnp.bfloat16), 'tp', scatter_dimension...  27.5 us
    reduce_scatter x1, waiting for transfers between devices, on_device(): lax.psum_scatter(down_term.astype(jnp.bfloat16), 'tp', scatter_dimension=...  26.5 us
    all_gather x1, waiting for transfers between devices, on_device(): lax.all_gather(key_weight, 'fs', axis=0, tiled=True)  26.4 us
  transfers between devices with their start and end apart: 12, of which 12 were waited for; matrix products, arithmetic and copies ran while one was open for 6% of the time, Pallas kernels for 0%

commit v1 on v0

--- a/solution.py
+++ b/solution.py
@@ -165,9 +165,24 @@
     )
     gathered_mid = lax.all_gather(middle, "tp", axis=1, tiled=True)
     normed_mid = rms_scale(gathered_mid, middle_gain)
+
+    def cover_the_ladders(matrix):
+        built = lax.psum(1, axis_name="fs")
+        mat_out = lax.axis_index("fs")
+        moved, small, big = (built, mat_out, matrix.shape[0])
+        block_list = [(c, (c + 1) % moved) for c in range(moved)]
+        oldest = matrix
+        mixed_arr = jnp.zeros((*matrix.shape[:0], moved * big, *matrix.shape[1:]), matrix.dtype)
+        for it in range(moved):
+            extra = (small - it) % moved
+            mixed_arr = lax.dynamic_update_slice_in_dim(mixed_arr, oldest, extra * big, axis=0)
+            if it < moved - 1:
+                oldest = lax.ppermute(oldest, axis_name="fs", perm=block_list)
+        return mixed_arr
+
     gate_full, up_full = (
         lax.all_gather(gate_weight, "fs", axis=0, tiled=True),
-        lax.all_gather(up_weight, "fs", axis=0, tiled=True),
+        cover_the_ladders(up_weight),
     )
     gate_act = jnp.dot(normed_mid, gate_full, preferred_element_type=jnp.float32)
     up_act = jnp.dot(normed_mid, up_full, preferred_element_type=jnp.float32)

time: 572 us -> 528 us (0.923)
  waiting for transfers between devices: 505 us -> 428 us
  starting transfers between devices: 0.61 us -> 29 us
  local copies, waits for them, and re-layouts: 5.47 us -> 12 us
    ppermute x0 -> x3, waiting for transfers between devices: none -> 138 us  [cover_the_ladders(): oldest = lax.ppermute(oldest, axis_name='fs', perm=block_list)]
    all_gather x1, waiting for transfers between devices: 97.8 us -> 0.02 us  [on_device(): lax.all_gather(gate_weight, 'fs', axis=0, tiled=True)]
    all_gather x1 -> x0, waiting for transfers between devices: 91.3 us -> none  [on_device(): lax.all_gather(up_weight, 'fs', axis=0, tiled=True)]
    ppermute x0 -> x3, starting transfers between devices: none -> 28.6 us  [cover_the_ladders(): oldest = lax.ppermute(oldest, axis_name='fs', perm=block_list)]
    all_gather x1, waiting for transfers between devices: 17.5 us -> 0.01 us  [on_device(): gathered_mid = lax.all_gather(middle, 'tp', axis=1, tiled=True)]
    all_gather x1, waiting for transfers between devices: 98 us -> 84.3 us  [on_device(): lax.all_gather(down_weight, 'fs', axis=1, tiled=True)]
    dynamic_update_slice x0 -> x4, local copies, waits for them, and re-layouts: none -> 7.31 us  [cover_the_ladders(): lax.dynamic_update_slice_in_dim(mixed_arr, oldest, extra * big, axis=0)]
  transfers between devices with their start and end apart: 12 -> 14, of which waited for: 12 -> 12; matrix products, arithmetic and copies ran while one was open for 6% -> 7% of each run, Pallas kernels for 0% -> 0%
where the time goes in v1:
time: 528 us; the launch traced here: 527 us
  waiting for transfers between devices  428 us (81%)
  matrix products  33.8 us (6%)
  starting transfers between devices  29 us (5%)
  between operations  13.6 us (3%)
  local copies, waits for them, and re-layouts  12 us (2%)
  other arithmetic  10.6 us (2%)
    ppermute x3, waiting for transfers between devices, cover_the_ladders(): oldest = lax.ppermute(oldest, axis_name='fs', perm=block_list)  138 us
    all_gather x1, waiting for transfers between devices, on_device(): lax.all_gather(down_weight, 'fs', axis=1, tiled=True)  84.3 us
    all_gather x1, waiting for transfers between devices, on_device(): lax.all_gather(merge_weight, 'fs', axis=1, tiled=True)  28.8 us
    ppermute x3, starting transfers between devices, cover_the_ladders(): oldest = lax.ppermute(oldest, axis_name='fs', perm=block_list)  28.6 us
    all_gather x1, waiting for transfers between devices, on_device(): lax.all_gather(query_weight, 'fs', axis=0, tiled=True)  27.7 us
    reduce_scatter x1, waiting for transfers between devices, on_device(): lax.psum_scatter(merge_term.astype(jnp.bfloat16), 'tp', scatter_dimension...  27.5 us
    reduce_scatter x1, waiting for transfers between devices, on_device(): lax.psum_scatter(down_term.astype(jnp.bfloat16), 'tp', scatter_dimension=...  26.5 us
    all_gather x1, waiting for transfers between devices, on_device(): lax.all_gather(key_weight, 'fs', axis=0, tiled=True)  26.4 us
  transfers between devices with their start and end apart: 14, of which 12 were waited for; matrix products, arithmetic and copies ran while one was open for 7% of the time, Pallas kernels for 0%

profile of v1, /device:TPU:0, one launch (start us, length us, event | category | flops | bytes accessed | tf_op | source)
XLA Modules:
  0.0 527.1 jit_solution(7453854581385990632)
XLA Ops:
  11.9 19.3 %all-gather.10.cloned.1.call-done = bf16[1,384,2048]{2,1,0:T(8,128)(2,1)} async-done(((bf16[1,384,512]{2,1,0:T(8,128)(2,1)}), bf16[1,384,2048]{2,1,0:T(8,128)(2,1)}) %all-gather.10.cloned.1.call-update) | async-done | bytes 1572880 | tf_op jit(solution)/shard_map/all_gather | solution.py:134
  31.3 1.9 fusion.3
  33.2 27.7 %all-gather.16.cloned.1.call-done = bf16[2048,256]{1,0:T(8,128)(2,1)} async-done(((bf16[512,256]{1,0:T(8,128)(2,1)}), bf16[2048,256]{1,0:T(8,128)(2,1)}) %all-gather.16.cloned.1.call-update) | async-done | bytes 1048592 | tf_op jit(solution)/shard_map/all_gather | solution.py:138
  60.9 2.6 convolution_convert_fusion.3
  63.5 26.4 %all-gather.18.cloned.1.call-done = bf16[2048,256]{1,0:T(8,128)(2,1)} async-done(((bf16[512,256]{1,0:T(8,128)(2,1)}), bf16[2048,256]{1,0:T(8,128)(2,1)}) %all-gather.18.cloned.1.call-update) | async-done | bytes 1048592 | tf_op jit(solution)/shard_map/all_gather | solution.py:139
  89.8 2.1 convolution_convert_fusion.2
  93.0 25.7 %all-gather.14.cloned.1.call-done = bf16[2048,256]{1,0:T(8,128)(2,1)} async-done(((bf16[512,256]{1,0:T(8,128)(2,1)}), bf16[2048,256]{1,0:T(8,128)(2,1)}) %all-gather.14.cloned.1.call-update) | async-done | bytes 1048592 | tf_op jit(solution)/shard_map/all_gather | solution.py:140
  118.6 1.9 convolution_convert_fusion.4
  128.5 18.9 %all-gather.12.cloned.1.call-done = bf16[2048,256]{1,0:T(8,128)(2,1)} async-done(((bf16[512,256]{1,0:T(8,128)(2,1)}), bf16[2048,256]{1,0:T(8,128)(2,1)}) %all-gather.12.cloned.1.call-update) | async-done | bytes 1048592 | tf_op jit(solution)/shard_map/all_gather | solution.py:141
  147.5 28.8 %all-gather.20.cloned.1.call-done = bf16[256,2048]{1,0:T(8,128)(2,1)} async-done(((bf16[256,512]{1,0:T(8,128)(2,1)}), bf16[256,2048]{1,0:T(8,128)(2,1)}) %all-gather.20.cloned.1.call-update) | async-done | bytes 1048592 | tf_op jit(solution)/shard_map/all_gather | solution.py:157
  176.3 4.6 convolution_convert_fusion.1
  180.9 27.5 %reduce-scatter.3.cloned.1.call-done = bf16[384,512]{1,0:T(8,128)(2,1)} async-done(((bf16[384,2048]{1,0:T(8,128)(2,1)}), bf16[384,512]{1,0:T(8,128)(2,1)}) %reduce-scatter.3.cloned.1.call-update) | async-done | bytes 393232 | tf_op jit(solution)/shard_map/reduce_scatter | solution.py:160
  208.4 1.8 fusion.12
  213.2 30.7 %collective-permute-done = bf16[512,1280]{1,0:T(8,128)(2,1)S(1)} collective-permute-done((bf16[512,1280]{1,0:T(8,128)(2,1)S(1)}, bf16[512,1280]{1,0:T(8,128)(2,1)S(1)}, u32[]{:S(2)}, u32[]{:S(2)}) %collective-permute-start) | collective-permute-done | bytes 1310752 | tf_op jit(solution)/shard_map/ppermute | solution.py:180
  244.1 60.8 %collective-permute-done.1 = bf16[512,1280]{1,0:T(8,128)(2,1)} collective-permute-done((bf16[512,1280]{1,0:T(8,128)(2,1)S(1)}, bf16[512,1280]{1,0:T(8,128)(2,1)}, u32[]{:S(2)}, u32[]{:S(2)}) %collective-permute-start.1) | collective-permute-done | bytes 1310752 | tf_op jit(solution)/shard_map/ppermute | solution.py:180
  304.9 26.9 %collective-permute-start.2 = (bf16[512,1280]{1,0:T(8,128)(2,1)}, bf16[512,1280]{1,0:T(8,128)(2,1)}, u32[]{:S(2)}, u32[]{:S(2)}) collective-permute-start(bf16[512,1280]{1,0:T(8,128)(2,1)} %collective-permute-done.1), channel_id=1, source_target_pairs={{0,4},{4,8},{8,12},{12,0},{1,5},{5,9},{9,13},{13,1},{2,6},{6,10},{... | collective-permute-start | bytes 3932168 | tf_op jit(solution)/shard_map/ppermute | solution.py:180
  331.8 2.6 broadcast_in_dim.30
  336.8 2.5 constant_dynamic-update-slice_fusion.3
  339.3 46.3 %collective-permute-done.2 = bf16[512,1280]{1,0:T(8,128)(2,1)} collective-permute-done((bf16[512,1280]{1,0:T(8,128)(2,1)}, bf16[512,1280]{1,0:T(8,128)(2,1)}, u32[]{:S(2)}, u32[]{:S(2)}) %collective-permute-start.2) | collective-permute-done | bytes 1310752 | tf_op jit(solution)/shard_map/ppermute | solution.py:180
  385.6 2.5 constant_dynamic-update-slice_fusion.2
  389.9 7.3 %fusion.15 = f32[384,1280]{1,0:T(8,128)} fusion(bf16[2048,1280]{1,0:T(8,128)(2,1)} %all-gather.24.cloned.1.call-done, bf16[384,2048]{1,0:T(8,128)(2,1)} %all-gather.22.cloned.1.call-done, f32[2048]{0:T(1024)S(1)} %copy-done.8, f32[384]{0:T(512)S(1)} %add_rsqrt_fusion), kind=kOutput, calls=%fused_computation.36 | convolution fusion | flops 2016411648 | bytes 8791552 | tf_op jit(solution)/shard_map/dot_general | solution.py:187
  397.1 84.3 %all-gather.26.cloned.1.call-done = bf16[1280,2048]{1,0:T(8,128)(2,1)} async-done(((bf16[1280,512]{1,0:T(8,128)(2,1)}), bf16[1280,2048]{1,0:T(8,128)(2,1)}) %all-gather.26.cloned.1.call-update) | async-done | bytes 5242896 | tf_op jit(solution)/shard_map/all_gather | solution.py:192
  481.5 10.7 %convolution_convert_fusion = bf16[384,2048]{1,0:T(8,128)(2,1)} fusion(bf16[1280,2048]{1,0:T(8,128)(2,1)} %all-gather.26.cloned.1.call-done, bf16[2048,1280]{1,0:T(8,128)(2,1)} %constant_dynamic-update-slice_fusion.2, f32[384,1280]{1,0:T(8,128)} %fusion.15, bf16[384,2048]{1,0:T(8,128)(2,1)S(1)} %copy-done.3, f32[2048]{0:T(1024)S(1)} %copy-done.8, ...), kind=kOutput, calls=%fused_computation.15 | convolution fusion | flops 4033413120 | bytes 15607296 | tf_op jit(solution)/shard_map/dot_general | solution.py:190
  492.2 26.5 %reduce-scatter.5.cloned.1.call-done = bf16[384,512]{1,0:T(8,128)(2,1)} async-done(((bf16[384,2048]{1,0:T(8,128)(2,1)}), bf16[384,512]{1,0:T(8,128)(2,1)}) %reduce-scatter.5.cloned.1.call-update) | async-done | bytes 393232 | tf_op jit(solution)/shard_map/reduce_scatter | solution.py:195
  (105 shorter events, 23.9 us)
Async XLA Ops:
  6.5 54.3 %copy-start.7 = (f32[2048]{0:T(1024)S(1)}, f32[2048]{0:T(1024)}, u32[]{:S(2)}) copy-start(f32[2048]{0:T(1024)} %param.18) | copy-start | bytes 24580
  6.5 24.7 %all-gather.10.cloned.1.call-start = ((), (), s32[]{:S(2)}) async-start(), calls=%async_computation.2 | async-start | bytes 1966080 | tf_op jit(solution)/shard_map/all_gather | solution.py:134
  7.3 53.6 %all-gather.16.cloned.1.call-start = ((), (), s32[]{:S(2)}) async-start(), calls=%async_computation.5 | async-start | bytes 1310720 | tf_op jit(solution)/shard_map/all_gather | solution.py:138
  8.0 81.8 %all-gather.18.cloned.1.call-start = ((), (), s32[]{:S(2)}) async-start(), calls=%async_computation.6 | async-start | bytes 1310720 | tf_op jit(solution)/shard_map/all_gather | solution.py:139
  8.7 109.9 %all-gather.14.cloned.1.call-start = ((), (), s32[]{:S(2)}) async-start(), calls=%async_computation.4 | async-start | bytes 1310720 | tf_op jit(solution)/shard_map/all_gather | solution.py:140
  9.3 138.1 %all-gather.12.cloned.1.call-start = ((), (), s32[]{:S(2)}) async-start(), calls=%async_computation.3 | async-start | bytes 1310720 | tf_op jit(solution)/shard_map/all_gather | solution.py:141
  9.9 166.4 %all-gather.20.cloned.1.call-start = ((), (), s32[]{:S(2)}) async-start(), calls=%async_computation.7 | async-start | bytes 1310720 | tf_op jit(solution)/shard_map/all_gather | solution.py:157
  10.5 197.9 %reduce-scatter.3.cloned.1.call-start = ((), (), s32[]{:S(2)}) async-start(), calls=%async_computation.8 | async-start | bytes 1966080 | tf_op jit(solution)/shard_map/reduce_scatter | solution.py:160
  31.3 58.6 %copy-start.1 = (bf16[1,384,2048]{2,1,0:T(8,128)(2,1)S(1)}, bf16[1,384,2048]{2,1,0:T(8,128)(2,1)}, u32[]{:S(2)}) copy-start(bf16[1,384,2048]{2,1,0:T(8,128)(2,1)} %all-gather.10.cloned.1.call-done) | copy-start | bytes 4718596
  121.0 1.2 copy-start.6
  126.3 50.0 %copy-start.2 = (bf16[1,384,2048]{2,1,0:T(8,128)(2,1)S(1)}, bf16[1,384,2048]{2,1,0:T(8,128)(2,1)}, u32[]{:S(2)}) copy-start(bf16[1,384,2048]{2,1,0:T(8,128)(2,1)} %all-gather.10.cloned.1.call-done) | copy-start | bytes 4718596
  128.5 79.9 %copy-start.4 = (bf16[1,384,512]{2,1,0:T(8,128)(2,1)S(1)}, bf16[1,384,512]{2,1,0:T(8,128)(2,1)}, u32[]{:S(2)}) copy-start(bf16[1,384,512]{2,1,0:T(8,128)(2,1)} %param.17) | copy-start | bytes 1179652
  180.9 30.8 %copy-start.5 = (bf16[512,1280]{1,0:T(8,128)(2,1)S(1)}, bf16[512,1280]{1,0:T(8,128)(2,1)}, u32[]{:S(2)}) copy-start(bf16[512,1280]{1,0:T(8,128)(2,1)} %param.28) | copy-start | bytes 3932164
  180.9 207.1 %all-gather.22.cloned.1.call-start = ((), (), s32[]{:S(2)}) async-start(), calls=%async_computation.9 | async-start | bytes 1966080 | tf_op jit(solution)/shard_map/all_gather | solution.py:166
  210.3 179.6 %all-gather.24.cloned.1.call-start = ((), (), s32[]{:S(2)}) async-start(), calls=%async_computation.10 | async-start | bytes 6553600 | tf_op jit(solution)/shard_map/all_gather | solution.py:184
  211.0 270.5 %all-gather.26.cloned.1.call-start = ((), (), s32[]{:S(2)}) async-start(), calls=%async_computation.11 | async-start | bytes 6553600 | tf_op jit(solution)/shard_map/all_gather | solution.py:192
  211.6 307.1 %reduce-scatter.5.cloned.1.call-start = ((), (), s32[]{:S(2)}) async-start(), calls=%async_computation.12 | async-start | bytes 1966080 | tf_op jit(solution)/shard_map/reduce_scatter | solution.py:195
  211.7 32.3 %collective-permute-start = (bf16[512,1280]{1,0:T(8,128)(2,1)S(1)}, bf16[512,1280]{1,0:T(8,128)(2,1)S(1)}, u32[]{:S(2)}, u32[]{:S(2)}) collective-permute-start(bf16[512,1280]{1,0:T(8,128)(2,1)S(1)} %copy-done.5), channel_id=1, source_target_pairs={{0,4},{4,8},{8,12},{12,0},{1,5},{5,9},{9,13},{13,1},{2,6},{6,10},{... | collective-permute-start | bytes 3932168 | tf_op jit(solution)/shard_map/ppermute | solution.py:180
  244.0 60.9 %collective-permute-start.1 = (bf16[512,1280]{1,0:T(8,128)(2,1)S(1)}, bf16[512,1280]{1,0:T(8,128)(2,1)}, u32[]{:S(2)}, u32[]{:S(2)}) collective-permute-start(bf16[512,1280]{1,0:T(8,128)(2,1)S(1)} %collective-permute-done), channel_id=1, source_target_pairs={{0,4},{4,8},{8,12},{12,0},{1,5},{5,9},{9,13},{13,1},{2,6},{6,10},{... | collective-permute-start | bytes 3932168 | tf_op jit(solution)/shard_map/ppermute | solution.py:180
  304.9 80.7 %collective-permute-start.2 = (bf16[512,1280]{1,0:T(8,128)(2,1)}, bf16[512,1280]{1,0:T(8,128)(2,1)}, u32[]{:S(2)}, u32[]{:S(2)}) collective-permute-start(bf16[512,1280]{1,0:T(8,128)(2,1)} %collective-permute-done.1), channel_id=1, source_target_pairs={{0,4},{4,8},{8,12},{12,0},{1,5},{5,9},{9,13},{13,1},{2,6},{6,10},{... | collective-permute-start | bytes 3932168 | tf_op jit(solution)/shard_map/ppermute | solution.py:180
  336.8 53.1 %copy-start.8 = (f32[2048]{0:T(1024)S(1)}, f32[2048]{0:T(1024)}, u32[]{:S(2)}) copy-start(f32[2048]{0:T(1024)} %param.26) | copy-start | bytes 24580
  389.8 91.7 %copy-start.3 = (bf16[384,2048]{1,0:T(8,128)(2,1)S(1)}, bf16[384,2048]{1,0:T(8,128)(2,1)}, u32[]{:S(2)}) copy-start(bf16[384,2048]{1,0:T(8,128)(2,1)} %all-gather.22.cloned.1.call-done) | copy-start | bytes 4718596
  397.1 121.6 %copy-start = (bf16[384,512]{1,0:T(8,128)(2,1)S(1)}, bf16[384,512]{1,0:T(8,128)(2,1)}, u32[]{:S(2)}) copy-start(bf16[384,512]{1,0:T(8,128)(2,1)} %fusion.12) | copy-start | bytes 1179652
Sparse Core Ops, SparseCore 0:
  8.9 22.3 all-gather.9
  32.8 27.9 all-gather.15
  62.4 27.3 all-gather.17
  91.3 27.3 all-gather.13
  120.1 27.3 all-gather.11
  148.9 27.3 all-gather.19
  181.0 27.3 reduce-scatter.2
  210.4 19.6 all-gather.21
  231.7 149.4 all-gather.23
  382.6 98.8 all-gather.25
  492.3 26.3 reduce-scatter.4
